TPU v7x, 32 devices: a whole 2x2x4 slice. The times are simulated.
32 devices in a mesh: grp: 2 (over y), ra: 4 (over z), cb: 4 (over x, core).
Axes of the slice: x: 2, y: 2, z: 4, core: 2. Of those that a mesh axis runs over, the one named last changes fastest.
Arguments:
- tokens: bfloat16 [256, 2048], P('grp', 'ra'), parts along dimension 0, may hold values from -8 to 8
- first_gain: bfloat16 [2048], P('ra'), may hold values from 0.099609375 to 1.8984375
- first_gate: bfloat16 [2048, 5632], P('ra', 'cb'), may hold values from -0.125 to 0.125
- first_up: bfloat16 [2048, 5632], P('ra', 'cb'), may hold values from -0.125 to 0.125
- first_down: bfloat16 [5632, 2048], P('cb', 'ra'), may hold values from -0.078125 to 0.078125
- second_gain: bfloat16 [2048], P('ra'), may hold values from 0.099609375 to 1.8984375
- second_gate: bfloat16 [2048, 5632], P('ra', 'cb'), may hold values from -0.125 to 0.125
- second_up: bfloat16 [2048, 5632], P('ra', 'cb'), may hold values from -0.125 to 0.125
- second_down: bfloat16 [5632, 2048], P('cb', 'ra'), may hold values from -0.078125 to 0.078125
Outputs:
- latent_out: bfloat16 [256, 2048], P('grp', 'ra'), parts along dimension 0
There are 2 independent parts, one for each index of `grp`. A program takes and returns all parts, laid end to end along the dimension named above; an argument that names none is the same for every part. Nothing has to cross between parts.
All inputs are finite; a program needn't handle non-finite values.
Results may differ from a plain program's by a relative error of at most 0.0088.
Values may be sent and summed in bfloat16 or wider, within the bound.
A program may use at most 64 MiB of HBM per device.

v0:
```python
import jax
import jax.numpy as jnp
from jax import lax
from jax.sharding import PartitionSpec as P


def sublayer(x, gain, w_gate, w_up, w_down):
    xf = x.astype(jnp.float32)
    width = x.shape[1] * lax.axis_size("ra")
    rows = x.shape[0]
    squares = jnp.sum(xf * xf, axis=1)
    normed = (xf * gain.astype(jnp.float32)).astype(jnp.bfloat16)
    dims = (((0,), (1,)), ((), ()))
    gate_rows = lax.dot_general(w_gate, normed, dims, preferred_element_type=jnp.float32)
    up_rows = lax.dot_general(w_up, normed, dims, preferred_element_type=jnp.float32)
    shares = lax.psum_scatter(
        jnp.concatenate([gate_rows, up_rows], axis=1), "ra", scatter_dimension=0, tiled=True
    )
    total_sq = lax.psum(squares, "ra")
    scale = lax.rsqrt(total_sq / width + 1e-06)
    hidden_t = (
        jax.nn.silu(shares[:, :rows] * scale[None, :]) * (shares[:, rows:] * scale[None, :])
    ).astype(jnp.bfloat16)
    partial_value = lax.dot_general(
        lax.all_gather(hidden_t, "ra", axis=0, tiled=True),
        w_down,
        (((0,), (0,)), ((), ())),
        preferred_element_type=jnp.float32,
    )
    branch = lax.psum(partial_value, "cb")
    return (0.5 * xf + 0.5 * branch).astype(jnp.bfloat16)


def per_device(
    tokens,
    first_gain,
    first_gate,
    first_up,
    first_down,
    second_gain,
    second_gate,
    second_up,
    second_down,
):
    middle = sublayer(tokens, first_gain, first_gate, first_up, first_down)
    return sublayer(middle, second_gain, second_gate, second_up, second_down)


def solution(mesh):
    placed = (
        P("grp", "ra"),
        P("ra"),
        P("ra", "cb"),
        P("ra", "cb"),
        P("cb", "ra"),
        P("ra"),
        P("ra", "cb"),
        P("ra", "cb"),
        P("cb", "ra"),
    )
    return jax.shard_map(
        per_device, mesh=mesh, in_specs=placed, out_specs=P("grp", "ra"), check_vma=False
    )
```

profile of v0, /device:TPU:0, one launch (start us, length us, event | category | flops | bytes accessed | tf_op | source)
XLA Modules:
  0.0 194.4 jit_solution(9216063514448310554)
XLA Ops:
  6.5 0.8 convert_element_type.31
  7.4 0.5 copy-done
  7.9 1.3 convolution_bitcast_fusion.2
  9.2 0.4 convolution_bitcast_fusion.3
  9.6 0.1 pad_maximum_fusion
  9.7 1.6 copy.12
  11.3 0.1 fusion.1
  11.5 13.6 %psum.28 = f32[128]{0:T(128)S(1)} all-reduce(f32[128]{0:T(128)S(1)} %fusion.1), channel_id=1, replica_groups=mesh['grp'=2,'ra'=4,'cb'=4] {'ra'}, use_global_device_ids=true, to_apply=%region_2.0 | all-reduce | flops 128 | bytes 1024 | tf_op jit(solution)/shard_map/psum | solution.py:19
  25.1 22.5 %reduce-scatter.7.cloned.1.call-done = f32[352,256]{1,0:T(8,128)} async-done(((f32[1408,256]{1,0:T(8,128)}), f32[352,256]{1,0:T(8,128)}) %reduce-scatter.7.cloned.1.call-update) | async-done | bytes 360464
  47.6 1.7 fusion.14
  49.3 0.1 copy.16
  49.4 1.1 copy.17
  50.5 0.1 multiply_convert_fusion.1
  50.6 0.1 copy.10
  50.8 15.0 %all_gather.6 = bf16[1408,128]{1,0:T(8,128)(2,1)S(1)} all-gather(bf16[352,128]{1,0:T(8,128)(2,1)S(1)} %copy.10), channel_id=1, replica_groups=mesh['grp'=2,'ra'=4,'cb'=4] {'ra'}, dimensions={0}, use_global_device_ids=true | all-gather | bytes 450560 | tf_op jit(solution)/shard_map/all_gather | solution.py:25
  65.8 1.1 fusion.15
  67.0 30.7 %all-reduce.3.cloned.1.call-done = f32[128,512]{1,0:T(8,128)} async-done(((f32[128,512]{1,0:T(8,128)}), f32[128,512]{1,0:T(8,128)}) %all-reduce.3.cloned.1.call-update) | async-done | bytes 262160 | tf_op jit(solution)/shard_map/psum | solution.py:30
  97.7 1.1 fusion.5
  98.8 1.7 convolution_bitcast_fusion
  100.5 0.4 convolution_bitcast_fusion.1
  101.0 1.6 copy.14
  102.6 12.1 %psum.30 = f32[128]{0:T(128)S(1)} all-reduce(f32[128]{0:T(128)S(1)} %get-tuple-element.5), channel_id=1, replica_groups=mesh['grp'=2,'ra'=4,'cb'=4] {'ra'}, use_global_device_ids=true, to_apply=%region_6.7 | all-reduce | flops 128 | bytes 1024 | tf_op jit(solution)/shard_map/psum | solution.py:19
  114.7 21.5 %reduce-scatter.9.cloned.1.call-done = f32[352,256]{1,0:T(8,128)} async-done(((f32[1408,256]{1,0:T(8,128)}), f32[352,256]{1,0:T(8,128)}) %reduce-scatter.9.cloned.1.call-update) | async-done | bytes 360464
  136.2 1.7 fusion.13
  137.9 0.1 copy.18
  138.0 1.1 copy.19
  139.1 0.1 multiply_convert_fusion
  139.2 0.1 copy.11
  139.3 15.1 %all_gather.7 = bf16[1408,128]{1,0:T(8,128)(2,1)S(1)} all-gather(bf16[352,128]{1,0:T(8,128)(2,1)S(1)} %copy.11), channel_id=1, replica_groups=mesh['grp'=2,'ra'=4,'cb'=4] {'ra'}, dimensions={0}, use_global_device_ids=true | all-gather | bytes 450560 | tf_op jit(solution)/shard_map/all_gather | solution.py:25
  154.4 1.1 fusion.16
  155.5 30.7 %all-reduce.5.cloned.1.call-done = f32[128,512]{1,0:T(8,128)} async-done(((f32[128,512]{1,0:T(8,128)}), f32[128,512]{1,0:T(8,128)}) %all-reduce.5.cloned.1.call-update) | async-done | bytes 262160 | tf_op jit(solution)/shard_map/psum | solution.py:30
  186.2 1.6 fusion.7
  (25 shorter events, 0.3 us)
Async XLA Ops:
  6.5 1.4 copy-start
  6.5 2.7 %copy-start.1 = (bf16[128,512]{1,0:T(8,128)(2,1)S(1)}, bf16[128,512]{1,0:T(8,128)(2,1)}, u32[]{:S(2)}) copy-start(bf16[128,512]{1,0:T(8,128)(2,1)} %param.9) | copy-start | bytes 393220
  6.5 2.7 %copy-start.2 = (bf16[512,1408]{1,0:T(8,128)(2,1)S(1)}, bf16[512,1408]{1,0:T(8,128)(2,1)}, u32[]{:S(2)}) copy-start(bf16[512,1408]{1,0:T(8,128)(2,1)} %param.11) | copy-start | bytes 4325380
  6.5 41.1 %reduce-scatter.7.cloned.1.call-start = ((), (), s32[]{:S(2)}) async-start(), calls=%async_computation.4 | async-start | bytes 1802240
  11.3 54.5 %copy-start.3 = (bf16[1408,512]{1,0:T(8,128)(2,1)S(1)}, bf16[1408,512]{1,0:T(8,128)(2,1)}, u32[]{:S(2)}) copy-start(bf16[1408,512]{1,0:T(8,128)(2,1)} %param.13) | copy-start | bytes 4325380
  11.3 86.4 %all-reduce.3.cloned.1.call-start = ((), (), s32[]{:S(2)}) async-start(), calls=%async_computation.2 | async-start | bytes 524288 | tf_op jit(solution)/shard_map/psum | solution.py:30
  50.6 16.3 %copy-start.6 = (bf16[512]{0:T(512)(128)(2,1)S(1)}, bf16[512]{0:T(512)(128)(2,1)}, u32[]{:S(2)}) copy-start(bf16[512]{0:T(512)(128)(2,1)} %param.14) | copy-start | bytes 3076
  66.9 33.6 %copy-start.4 = (bf16[512,1408]{1,0:T(8,128)(2,1)S(1)}, bf16[512,1408]{1,0:T(8,128)(2,1)}, u32[]{:S(2)}) copy-start(bf16[512,1408]{1,0:T(8,128)(2,1)} %param.15) | copy-start | bytes 4325380
  66.9 69.3 %reduce-scatter.9.cloned.1.call-start = ((), (), s32[]{:S(2)}) async-start(), calls=%async_computation.5 | async-start | bytes 1802240
  102.6 51.8 %copy-start.5 = (bf16[1408,512]{1,0:T(8,128)(2,1)S(1)}, bf16[1408,512]{1,0:T(8,128)(2,1)}, u32[]{:S(2)}) copy-start(bf16[1408,512]{1,0:T(8,128)(2,1)} %param.17) | copy-start | bytes 4325380
  102.6 83.6 %all-reduce.5.cloned.1.call-start = ((), (), s32[]{:S(2)}) async-start(), calls=%async_computation.3 | async-start | bytes 524288 | tf_op jit(solution)/shard_map/psum | solution.py:30
Sparse Core Ops, SparseCore 0:
  11.4 36.1 reduce-scatter.6
  67.0 30.5 all-reduce.2
  102.7 33.4 reduce-scatter.8
  155.7 30.5 all-reduce.4
where the time goes:
time: 195 us; the launch traced here: 194 us
  waiting for transfers between devices  105 us (54%)
  blocking collectives  55.8 us (29%)
  between operations  13.3 us (7%)
  local copies, waits for them, and re-layouts  9.67 us (5%)
  matrix products  6.01 us (3%)
  other arithmetic  4.14 us (2%)
    psum x2, waiting for transfers between devices, sublayer(): branch = lax.psum(partial_value, 'cb')  61.4 us
    unnamed x6, waiting for transfers between devices  44 us
    all_gather x2, blocking collectives, sublayer(): lax.all_gather(hidden_t, 'ra', axis=0, tiled=True)  30.1 us
    psum x2, blocking collectives, sublayer(): total_sq = lax.psum(squares, 'ra')  25.7 us
    unnamed x20, local copies, waits for them, and re-layouts  6.04 us
  transfers between devices with their start and end apart: 4, of which 4 were waited for; matrix products, arithmetic and copies ran while one was open for 0% of the time, Pallas kernels for 0%

commit v1 on v0

v1 whole, which is shorter than its diff:
```python
import functools

import jax
import jax.numpy as jnp
from jax import lax
from jax.experimental import pallas as pl
from jax.experimental.pallas import tpu as pltpu
from jax.sharding import PartitionSpec as P

MESH = pl.DeviceIdType.MESH
F32 = jnp.float32
BF16 = jnp.bfloat16
LAG = 4


def kernel(
    n, m, chunks, w, wp, pieces, half, width,
    x_ref, gain1, gate1, up1, down1, gain2, gate2, up2, down2, o_ref,
    xs, normed, wgu, wdn, send, recv, hid, sq_own, sq_in, sc, acc, r1, slots,
    w_sem, d_sem, send_sem, recv_sem, sq_send, sq_recv, dir_send, rel_send, hid_recv,
    core_send, core_recv, x_send, x_recv, mid_send, mid_recv,
):
    r = lax.axis_index("ra")
    b = lax.axis_index("cb")
    k0 = lax.rem(b, 2)
    xi = lax.div(b, 2)
    nx = m // 2
    sib = xi * 2 + 1 - k0
    odd = list(range(1, n, 2))
    cols = normed.shape[-1]
    pc = cols // pieces
    gains = (gain1, gain2)
    pos = (r, n - 1 - r)
    step = (1, -1)

    def place(d, p):
        return p if d == 0 else n - 1 - p

    def gate_copies(s, c):
        at = pl.ds(pl.multiple_of(c * w, w), w)
        g, u = ((gate1, up1), (gate2, up2))[s]
        return (
            pltpu.make_async_copy(g.at[:, at], wgu.at[s, c, :, pl.ds(0, w)], w_sem.at[s, c]),
            pltpu.make_async_copy(u.at[:, at], wgu.at[s, c, :, pl.ds(wp, w)], w_sem.at[s, c]),
        )

    def down_copy(s):
        return pltpu.make_async_copy((down1, down2)[s], wdn.at[s], d_sem.at[s])

    for s in range(2):
        @pl.loop(0, chunks)
        def _(c):
            for copy in gate_copies(s, c):
                copy.start()
        down_copy(s).start()

    barrier = pltpu.get_barrier_semaphore()
    for o in range(1, n):
        pl.semaphore_signal(barrier, 1, device_id={"ra": lax.rem(r + o, n)}, device_id_type=MESH)
    pl.semaphore_signal(barrier, 1, device_id={"cb": sib}, device_id_type=MESH)
    for o in range(1, nx):
        pl.semaphore_signal(
            barrier, 1, device_id={"cb": lax.rem(xi + o, nx) * 2 + k0}, device_id_type=MESH
        )

    for j in range(pieces):
        for d in range(2):
            xs[0, j, d] = x_ref[d * half:(d + 1) * half, j * pc:(j + 1) * pc]

    def remote(src, dst, ss, rs, where):
        return pltpu.make_async_remote_copy(
            src_ref=src, dst_ref=dst, send_sem=ss, recv_sem=rs, device_id=where, device_id_type=MESH
        )

    def sum_copy(s, d, c):
        return remote(send.at[s, d, c], recv.at[s, d, c], send_sem.at[s, d], recv_sem.at[s, d, c],
                      {"ra": r + step[d]})

    def hid_copy(s, d, c, ss, q):
        ref = hid.at[s, c, d]
        return remote(ref, ref, ss, hid_recv.at[s, d, c], {"ra": place(d, n - 1 - q)})

    def sq_copy(s, d, p):
        return remote(sq_own.at[s, d], sq_in.at[s, d, p], sq_send.at[s, d], sq_recv.at[s, d, p],
                      {"ra": place(d, n - 1)})

    def core_copy(s, j):
        return remote(acc.at[s, 1 - k0, j], r1.at[s, j], core_send.at[s, j], core_recv.at[s, j],
                      {"cb": sib})

    def x_copy(s, j, o):
        ref = slots.at[s, xi, j]
        return remote(ref, ref, x_send.at[s, o - 1, j], x_recv.at[s, o - 1, j],
                      {"cb": lax.rem(xi + o, nx) * 2 + k0})

    def mid_copy(s, j):
        ref = xs.at[s + 1, j, k0]
        return remote(ref, ref, mid_send.at[s, j], mid_recv.at[s, j], {"cb": sib})

    lane = lax.broadcasted_iota(jnp.int32, (8, 128), 1)
    for s in range(2):
        for d in range(2):
            total = jnp.zeros((half, 1), F32)
            for j in range(pieces):
                at = slice(j * pc, (j + 1) * pc)
                xf = xs[s, j, d].astype(F32)
                total = total + jnp.sum(xf * xf, axis=1, keepdims=True)
                normed[s, d, :, at] = (xf * gains[s][:, at].astype(F32)).astype(BF16)
            packed = jnp.zeros((8, 128), F32)
            for g in range(half // 8):
                packed = jnp.where(lane == g, total[g * 8:(g + 1) * 8], packed)
            sq_own[s, d] = packed
        if s == 0:
            pl.semaphore_wait(barrier, n - 1 + nx)
        for d in range(2):
            @pl.when(pos[d] < n - 1)
            def _():
                sq_copy(s, d, pos[d]).start()

        @pl.loop(0, chunks + LAG * n)
        def _(i):
            first = i - LAG * jnp.minimum(pos[0], pos[1])

            @pl.when((first >= 0) & (first < chunks))
            def _():
                whole = wgu.at[s, first, :, pl.ds(0, 2 * w)]
                pltpu.make_async_copy(whole, whole, w_sem.at[s, first]).wait()

            for d in range(2):
                c = i - LAG * pos[d]

                @pl.when((c >= 0) & (c < chunks))
                def _():
                    share = jnp.dot(normed[s, d], wgu[s, c], preferred_element_type=F32)

                    @pl.when(pos[d] == 0)
                    def _():
                        send[s, d, c] = share.astype(BF16)

                    @pl.when((pos[d] > 0) & (pos[d] < n - 1))
                    def _():
                        sum_copy(s, d, c).wait_recv()
                        send[s, d, c] = (share + recv[s, d, c].astype(F32)).astype(BF16)

                    @pl.when(pos[d] < n - 1)
                    def _():
                        sum_copy(s, d, c).start()

                    @pl.when(pos[d] == n - 1)
                    def _():
                        @pl.when(c == 0)
                        def _():
                            packed = sq_own[s, d]
                            for p in range(n - 1):
                                sq_copy(s, d, p).wait_recv()
                                packed = packed + sq_in[s, d, p]
                            packed = lax.rsqrt(packed / width + 1e-06)
                            for g in range(half // 8):
                                sc[s, d, g * 8:(g + 1) * 8] = jnp.broadcast_to(
                                    packed[:, g:g + 1], (8, 128)
                                )

                        sum_copy(s, d, c).wait_recv()
                        pre = share + recv[s, d, c].astype(F32)
                        scale = sc[s, d][:, :1]
                        gate = pre[:, :w] * scale
                        up = pre[:, wp:wp + w] * scale
                        hid[s, c, d] = (gate / (1.0 + jnp.exp(-gate)) * up).astype(BF16)
                        for t, q in enumerate(odd):
                            hid_copy(s, d, c, dir_send.at[s, d, t], q).start()

                back = n - 1 - pos[d]
                e = i - LAG * n

                @pl.when((lax.rem(back, 2) == 1) & (back < n - 1) & (e >= 0))
                def _():
                    hid_copy(s, d, e, rel_send.at[s, d], back + 1).wait_recv()
                    hid_copy(s, d, e, rel_send.at[s, d], back + 1).start()

        down_copy(s).wait()
        for j in range(pieces):
            for d in range(2):
                acc[s, d, j] = jnp.zeros((half, pc), F32)

        @pl.loop(0, chunks)
        def _(c):
            for d in range(2):
                back = n - 1 - pos[d]

                @pl.when((back > 0) & ((lax.rem(back, 2) == 0) | (back == n - 1)))
                def _():
                    hid_copy(s, d, c, rel_send.at[s, d], 1).wait_recv()

            rows = hid[s, c].reshape(2 * half, w)
            for j in range(pieces):
                out = jnp.dot(rows, wdn[s, c, :, j * pc:(j + 1) * pc], preferred_element_type=F32)
                for d in range(2):
                    acc[s, d, j] = acc[s, d, j] + out[d * half:(d + 1) * half]

        for j in range(pieces):
            core_copy(s, j).start()
        for j in range(pieces):
            core_copy(s, j).wait_recv()
            slots[s, xi, j] = (acc[s, k0, j] + r1[s, j]).astype(BF16)
            for o in range(1, nx):
                x_copy(s, j, o).start()
        for j in range(pieces):
            for o in range(1, nx):
                x_copy(s, j, o).wait_recv()
            branch = slots[s, 0, j].astype(F32)
            for o in range(1, nx):
                branch = branch + slots[s, o, j].astype(F32)
            xs[s + 1, j, k0] = (0.5 * xs[s, j, k0].astype(F32) + 0.5 * branch).astype(BF16)
            mid_copy(s, j).start()
        for j in range(pieces):
            mid_copy(s, j).wait_recv()

    for j in range(pieces):
        for d in range(2):
            o_ref[d * half:(d + 1) * half, j * pc:(j + 1) * pc] = xs[2, j, d]

    for s in range(2):
        for d in range(2):
            @pl.when(pos[d] < n - 1)
            def _():
                sq_copy(s, d, 0).wait_send()
                remote(send.at[s, d], recv.at[s, d], send_sem.at[s, d], recv_sem.at[s, d, 0],
                       {"ra": r + step[d]}).wait_send()

            ref = hid.at[s, :, d]

            @pl.when(pos[d] == n - 1)
            def _():
                for t, q in enumerate(odd):
                    remote(ref, ref, dir_send.at[s, d, t], hid_recv.at[s, d, 0],
                           {"ra": place(d, n - 1 - q)}).wait_send()

            back = n - 1 - pos[d]

            @pl.when((lax.rem(back, 2) == 1) & (back < n - 1))
            def _():
                remote(ref, ref, rel_send.at[s, d], hid_recv.at[s, d, 0],
                       {"ra": place(d, n - 2 - back)}).wait_send()

        for j in range(pieces):
            core_copy(s, j).wait_send()
            mid_copy(s, j).wait_send()
            for o in range(1, nx):
                x_copy(s, j, o).wait_send()


def per_device(n, m, x, gain1, gate1, up1, down1, gain2, gate2, up2, down2):
    rows, cols = x.shape
    ff = gate1.shape[1]
    w = wp = 128
    chunks = -(-ff // w)
    ragged = chunks * w - ff
    if ragged:
        gate1, up1, gate2, up2 = (
            jnp.pad(a, ((0, 0), (0, ragged))) for a in (gate1, up1, gate2, up2)
        )
        down1, down2 = (jnp.pad(a, ((0, ragged), (0, 0))) for a in (down1, down2))
    pieces = 2 if cols % 256 == 0 else 1
    half = rows // 2
    pc = cols // pieces
    odd = n // 2
    nx = m // 2
    vmem = pl.BlockSpec(memory_space=pltpu.VMEM)
    hbm = pl.BlockSpec(memory_space=pl.ANY)
    dma = pltpu.SemaphoreType.DMA
    return pl.pallas_call(
        functools.partial(kernel, n, m, chunks, w, wp, pieces, half, cols * n),
        out_shape=jax.ShapeDtypeStruct((rows, cols), BF16),
        in_specs=[vmem, vmem, hbm, hbm, hbm, vmem, hbm, hbm, hbm],
        out_specs=vmem,
        scratch_shapes=[
            pltpu.VMEM((3, pieces, 2, half, pc), BF16),
            pltpu.VMEM((2, 2, half, cols), BF16),
            pltpu.VMEM((2, chunks, cols, 2 * wp), BF16),
            pltpu.VMEM((2, chunks, w, cols), BF16),
            pltpu.VMEM((2, 2, chunks, half, 2 * wp), BF16),
            pltpu.VMEM((2, 2, chunks, half, 2 * wp), BF16),
            pltpu.VMEM((2, chunks, 2, half, w), BF16),
            pltpu.VMEM((2, 2, 8, 128), F32),
            pltpu.VMEM((2, 2, n, 8, 128), F32),
            pltpu.VMEM((2, 2, half, 128), F32),
            pltpu.VMEM((2, 2, pieces, half, pc), F32),
            pltpu.VMEM((2, pieces, half, pc), F32),
            pltpu.VMEM((2, nx, pieces, half, pc), BF16),
            dma((2, chunks)), dma((2,)),
            dma((2, 2)), dma((2, 2, chunks)),
            dma((2, 2)), dma((2, 2, n)),
            dma((2, 2, odd)), dma((2, 2)), dma((2, 2, chunks)),
            dma((2, pieces)), dma((2, pieces)),
            dma((2, max(nx - 1, 1), pieces)), dma((2, max(nx - 1, 1), pieces)),
            dma((2, pieces)), dma((2, pieces)),
        ],
        compiler_params=pltpu.CompilerParams(collective_id=0, has_side_effects=True),
    )(
        x, gain1.reshape(1, cols), gate1, up1, down1.reshape(chunks, w, cols),
        gain2.reshape(1, cols), gate2, up2, down2.reshape(chunks, w, cols),
    )


def solution(mesh):
    placed = (
        P("grp", "ra"),
        P("ra"),
        P("ra", "cb"),
        P("ra", "cb"),
        P("cb", "ra"),
        P("ra"),
        P("ra", "cb"),
        P("ra", "cb"),
        P("cb", "ra"),
    )
    body = functools.partial(per_device, mesh.shape["ra"], mesh.shape["cb"])
    return jax.shard_map(
        body, mesh=mesh, in_specs=placed, out_specs=P("grp", "ra"), check_vma=False
    )
```

time: 195 us -> 66.9 us (0.34)
  waiting for transfers between devices: 105 us -> 0 us
  Pallas kernels: 0 us -> 61.7 us
  blocking collectives: 55.8 us -> 0 us
  between operations: 13.3 us -> 0.01 us
  matrix products: 6.01 us -> 0 us
  local copies, waits for them, and re-layouts: 9.67 us -> 4.09 us
  other arithmetic: 4.14 us -> 0 us
    pallas_call x0 -> x1, Pallas kernels: none -> 61.7 us  [per_device(): pl.pallas_call(functools.partial(kernel, n, m, chunks, w, wp, pieces, hal...]
    psum x2 -> x0, waiting for transfers between devices: 61.4 us -> none  [sublayer(): branch = lax.psum(partial_value, 'cb')]
    unnamed x6 -> x0, waiting for transfers between devices: 44 us -> none
    all_gather x2 -> x0, blocking collectives: 30.1 us -> none  [sublayer(): lax.all_gather(hidden_t, 'ra', axis=0, tiled=True)]
    psum x2 -> x0, blocking collectives: 25.7 us -> none  [sublayer(): total_sq = lax.psum(squares, 'ra')]
    dot_general x6 -> x0, matrix products: 6.01 us -> none  [the longest x2 3.02 us: sublayer(): lax.dot_general(w_up, normed, dims, preferred_element_type=jnp.float32)]
    unnamed x20 -> x1, local copies, waits for them, and re-layouts: 6.04 us -> 1.57 us
    slice x2 -> x0, local copies, waits for them, and re-layouts: 3.39 us -> none  [sublayer(): shares[:, :rows] * scale[None, :]]
  transfers between devices with their start and end apart: 4 -> 0, of which waited for: 4 -> 0; matrix products, arithmetic and copies ran while one was open for 0% -> 0% of each run, Pallas kernels for 0% -> 0%
where the time goes in v1:
time: 66.9 us; the launch traced here: 65.8 us
  Pallas kernels  61.7 us (92%)
  local copies, waits for them, and re-layouts  4.09 us (6%)
    pallas_call x1, Pallas kernels, per_device(): pl.pallas_call(functools.partial(kernel, n, m, chunks, w, wp, pieces, hal...  61.7 us
    unnamed x1, local copies, waits for them, and re-layouts  1.57 us

profile of v1, /device:TPU:0, one launch (start us, length us, event | category | flops | bytes accessed | tf_op | source)
XLA Modules:
  0.0 65.8 jit_solution(15697629140248900814)
XLA Ops:
  0.0 1.3 %reshape.12.gain1 = bf16[1,512]{1,0:T(2,128)(2,1)} reshape(bf16[512]{0:T(512)(128)(2,1)} %param.10) | data formatting | bytes 2048 | tf_op jit(solution)/shard_map/reshape | solution.py:300
  1.3 1.3 %reshape.14.gain2 = bf16[1,512]{1,0:T(2,128)(2,1)} reshape(bf16[512]{0:T(512)(128)(2,1)} %param.14) | data formatting | bytes 2048 | tf_op jit(solution)/shard_map/reshape | solution.py:301
  2.5 61.7 %shard_map.91 = bf16[128,512]{1,0:T(8,128)(2,1)} custom-call(bf16[128,512]{1,0:T(8,128)(2,1)} %x_ref.1, bf16[1,512]{1,0:T(2,128)(2,1)} %reshape.12.gain1, bf16[512,1408]{1,0:T(8,128)(2,1)} %gate1.1, bf16[512,1408]{1,0:T(8,128)(2,1)} %up1.1, bf16[11,128,512]{2,1,0:T(8,128)(2,1)} %bitcast.2, bf16[1,512]{1,0:T(2,128)(2,1)} %reshape.14.gain2, ...), custom_call_target="tpu_custom_call" | custom-call | tf_op jit(solution)/shard_map/pallas_call | solution.py:271
  64.3 1.6 %copy.11 = bf16[128,512]{1,0:T(8,128)(2,1)} copy(bf16[128,512]{1,0:T(8,128)(2,1)} %shard_map.91) | data formatting | bytes 262144

commit v2 on v1

v2 whole, which is shorter than its diff:
```python
import functools

import jax
import jax.numpy as jnp
from jax import lax
from jax.experimental import pallas as pl
from jax.experimental.pallas import tpu as pltpu
from jax.sharding import PartitionSpec as P

MESH = pl.DeviceIdType.MESH
F32 = jnp.float32
BF16 = jnp.bfloat16
LAG = 4


def kernel(
    n, m, chunks, w, half, width,
    x_ref, gain1, gate1, up1, down1, gain2, gate2, up2, down2, o_ref,
    xs, normed, wgu, wdn, send, recv, hid, sq_own, sq_in, sc, acc, r1, slots,
    w_sem, d_sem, send_sem, recv_sem, sq_send, sq_recv, dir_send, rel_send, hid_recv,
    core_send, core_recv, x_send, x_recv, mid_send, mid_recv,
):
    r = lax.axis_index("ra")
    b = lax.axis_index("cb")
    k0 = lax.rem(b, 2)
    xi = lax.div(b, 2)
    nx = m // 2
    sib = xi * 2 + 1 - k0
    odd = list(range(1, n, 2))
    quarter = half // 2
    gains = (gain1, gain2)

    def along(s, d, p):
        flip = d if s == 0 else 1 - d
        return p + flip * (n - 1 - 2 * p)

    def pos(s, d):
        return along(s, d, r)

    def gate_copies(s, c):
        at = pl.ds(pl.multiple_of(c * w, w), w)
        g, u = ((gate1, up1), (gate2, up2))[s]
        return (
            pltpu.make_async_copy(g.at[:, at], wgu.at[s, c, :, pl.ds(0, w)], w_sem.at[s, c]),
            pltpu.make_async_copy(u.at[:, at], wgu.at[s, c, :, pl.ds(w, w)], w_sem.at[s, c]),
        )

    def down_copy(s):
        return pltpu.make_async_copy((down1, down2)[s], wdn.at[s], d_sem.at[s])

    for s in range(2):
        @pl.loop(0, chunks)
        def _(c):
            for copy in gate_copies(s, c):
                copy.start()
        down_copy(s).start()

    barrier = pltpu.get_barrier_semaphore()
    for o in range(1, n):
        pl.semaphore_signal(barrier, 1, device_id={"ra": lax.rem(r + o, n)}, device_id_type=MESH)
    pl.semaphore_signal(barrier, 1, device_id={"cb": sib}, device_id_type=MESH)
    for o in range(1, nx):
        pl.semaphore_signal(
            barrier, 1, device_id={"cb": lax.rem(xi + o, nx) * 2 + k0}, device_id_type=MESH
        )

    for d in range(2):
        for t in range(2):
            at = d * half + t * quarter
            xs[0, d, t] = x_ref[at:at + quarter]

    def remote(src, dst, ss, rs, where):
        return pltpu.make_async_remote_copy(
            src_ref=src, dst_ref=dst, send_sem=ss, recv_sem=rs, device_id=where, device_id_type=MESH
        )

    def sum_copy(s, d, c):
        return remote(send.at[s, d, c], recv.at[s, d, c], send_sem.at[s, d], recv_sem.at[s, d, c],
                      {"ra": along(s, d, pos(s, d) + 1)})

    def hid_copy(s, d, c, ss, q):
        ref = hid.at[s, d, c]
        return remote(ref, ref, ss, hid_recv.at[s, d, c], {"ra": along(s, d, n - 1 - q)})

    def sq_copy(s, d, p):
        return remote(sq_own.at[s, d], sq_in.at[s, d, p], sq_send.at[s, d], sq_recv.at[s, d, p],
                      {"ra": along(s, d, n - 1)})

    def core_copy(s, d):
        return remote(acc.at[s, d, 1 - k0], r1.at[s, d], core_send.at[s, d], core_recv.at[s, d],
                      {"cb": sib})

    def x_copy(s, d, o):
        ref = slots.at[s, xi, d]
        return remote(ref, ref, x_send.at[s, o - 1, d], x_recv.at[s, o - 1, d],
                      {"cb": lax.rem(xi + o, nx) * 2 + k0})

    def mid_copy(s, d):
        ref = xs.at[s + 1, d, k0]
        return remote(ref, ref, mid_send.at[s, d], mid_recv.at[s, d], {"cb": sib})

    lane = lax.broadcasted_iota(jnp.int32, (8, 128), 1)

    def norm(s, d):
        gain = gains[s][...].astype(F32)[None, :]
        packed = jnp.zeros((8, 128), F32)
        for t in range(2):
            xf = xs[s, d, t].astype(F32)
            total = jnp.sum(xf * xf, axis=1, keepdims=True)
            normed[s, d, t * quarter:(t + 1) * quarter] = (xf * gain).astype(BF16)
            for g in range(quarter // 8):
                packed = jnp.where(lane == t * (quarter // 8) + g, total[g * 8:(g + 1) * 8], packed)
        sq_own[s, d] = packed

    def greet(s, d):
        @pl.when(pos(s, d) < n - 1)
        def _():
            sq_copy(s, d, pos(s, d)).start()

    def down(s, d):
        back = n - 1 - pos(s, d)
        cuts = sorted({0, max(chunks - 5, 0), max(chunks - 2, 0), chunks})
        for lo, hi in zip(cuts, cuts[1:]):
            @pl.when((back > 0) & ((lax.rem(back, 2) == 0) | (back == n - 1)))
            def _():
                for c in range(lo, hi):
                    hid_copy(s, d, c, rel_send.at[s, d], 1).wait_recv()

            rows = jnp.concatenate([hid[s, d, c] for c in range(lo, hi)], axis=1)
            out = jnp.dot(
                rows, wdn[s, lo:hi].reshape((hi - lo) * w, wdn.shape[-1]), preferred_element_type=F32
            )
            for t in range(2):
                part = out[t * quarter:(t + 1) * quarter]
                acc[s, d, t] = part if lo == 0 else acc[s, d, t] + part

        core_copy(s, d).start()

    def pair(s, d):
        core_copy(s, d).wait_recv()
        slots[s, xi, d] = (acc[s, d, k0] + r1[s, d]).astype(BF16)
        for o in range(1, nx):
            x_copy(s, d, o).start()

    def cross(s, d):
        for o in range(1, nx):
            x_copy(s, d, o).wait_recv()
        branch = slots[s, 0, d].astype(F32)
        for o in range(1, nx):
            branch = branch + slots[s, o, d].astype(F32)
        xs[s + 1, d, k0] = (0.5 * xs[s, d, k0].astype(F32) + 0.5 * branch).astype(BF16)
        mid_copy(s, d).start()

    def finish(s, d):
        mid_copy(s, d).wait_recv()
        if s == 0:
            norm(1, d)
            greet(1, d)

    near = jnp.where(2 * r >= n, 0, 1)
    edge = (r == 0) | (r == n - 1)

    def single(s, d):
        down(s, d)
        pair(s, d)
        cross(s, d)
        finish(s, d)

    def both(s, f):
        down(s, f)
        pair(s, f)
        down(s, 1 - f)
        cross(s, f)
        pair(s, 1 - f)
        finish(s, f)
        cross(s, 1 - f)
        finish(s, 1 - f)

    for s in range(2):
        if s == 0:
            for d in range(2):
                norm(0, d)
            pl.semaphore_wait(barrier, n - 1 + nx)
            for d in range(2):
                greet(0, d)
        else:
            @pl.when(edge)
            def _():
                single(0, near)

            @pl.when(jnp.logical_not(edge))
            def _():
                both(0, near)

        @pl.loop(0, chunks + LAG * n)
        def _(i):
            if s == 1:
                @pl.when(edge & (i == LAG * (n - 1)))
                def _():
                    single(0, 1 - near)

            first = i - LAG * jnp.minimum(r, n - 1 - r)

            @pl.when((first >= 0) & (first < chunks))
            def _():
                whole = wgu.at[s, first]
                pltpu.make_async_copy(whole, whole, w_sem.at[s, first]).wait()

            for d in range(2):
                at = pos(s, d)
                c = i - LAG * at

                @pl.when((c >= 0) & (c < chunks))
                def _():
                    share = jnp.dot(normed[s, d], wgu[s, c], preferred_element_type=F32)

                    @pl.when(at == 0)
                    def _():
                        send[s, d, c] = share.astype(BF16)

                    @pl.when((at > 0) & (at < n - 1))
                    def _():
                        sum_copy(s, d, c).wait_recv()
                        send[s, d, c] = (share + recv[s, d, c].astype(F32)).astype(BF16)

                    @pl.when(at < n - 1)
                    def _():
                        sum_copy(s, d, c).start()

                    @pl.when(at == n - 1)
                    def _():
                        @pl.when(c == 0)
                        def _():
                            packed = sq_own[s, d]
                            for p in range(n - 1):
                                sq_copy(s, d, p).wait_recv()
                                packed = packed + sq_in[s, d, p]
                            packed = lax.rsqrt(packed / width + 1e-06)
                            for g in range(half // 8):
                                sc[s, d, g * 8:(g + 1) * 8] = jnp.broadcast_to(
                                    packed[:, g:g + 1], (8, 128)
                                )

                        sum_copy(s, d, c).wait_recv()
                        pre = share + recv[s, d, c].astype(F32)
                        scale = sc[s, d]
                        gate = pre[:, :w] * scale
                        up = pre[:, w:] * scale
                        hid[s, d, c] = (gate / (1.0 + jnp.exp(-gate)) * up).astype(BF16)
                        for t, q in enumerate(odd):
                            hid_copy(s, d, c, dir_send.at[s, d, t], q).start()

                back = n - 1 - at
                e = i - LAG * n

                @pl.when((lax.rem(back, 2) == 1) & (back < n - 1) & (e >= 0))
                def _():
                    hid_copy(s, d, e, rel_send.at[s, d], back + 1).wait_recv()
                    hid_copy(s, d, e, rel_send.at[s, d], back + 1).start()

        down_copy(s).wait()

    both(1, 1 - near)

    for d in range(2):
        for t in range(2):
            at = d * half + t * quarter
            o_ref[at:at + quarter] = xs[2, d, t]

    for s in range(2):
        for d in range(2):
            at = pos(s, d)

            @pl.when(at < n - 1)
            def _():
                sq_copy(s, d, 0).wait_send()
                remote(send.at[s, d], recv.at[s, d], send_sem.at[s, d], recv_sem.at[s, d, 0],
                       {"ra": along(s, d, at + 1)}).wait_send()

            ref = hid.at[s, d]

            @pl.when(at == n - 1)
            def _():
                for t, q in enumerate(odd):
                    remote(ref, ref, dir_send.at[s, d, t], hid_recv.at[s, d, 0],
                           {"ra": along(s, d, n - 1 - q)}).wait_send()

            back = n - 1 - at

            @pl.when((lax.rem(back, 2) == 1) & (back < n - 1))
            def _():
                remote(ref, ref, rel_send.at[s, d], hid_recv.at[s, d, 0],
                       {"ra": along(s, d, at - 1)}).wait_send()

            core_copy(s, d).wait_send()
            mid_copy(s, d).wait_send()
            for o in range(1, nx):
                x_copy(s, d, o).wait_send()


def per_device(n, m, x, gain1, gate1, up1, down1, gain2, gate2, up2, down2):
    rows, cols = x.shape
    ff = gate1.shape[1]
    w = 128
    chunks = -(-ff // w)
    ragged = chunks * w - ff
    if ragged:
        gate1, up1, gate2, up2 = (
            jnp.pad(a, ((0, 0), (0, ragged))) for a in (gate1, up1, gate2, up2)
        )
        down1, down2 = (jnp.pad(a, ((0, ragged), (0, 0))) for a in (down1, down2))
    half = rows // 2
    quarter = half // 2
    odd = n // 2
    nx = m // 2
    vmem = pl.BlockSpec(memory_space=pltpu.VMEM)
    hbm = pl.BlockSpec(memory_space=pl.ANY)
    dma = pltpu.SemaphoreType.DMA
    return pl.pallas_call(
        functools.partial(kernel, n, m, chunks, w, half, cols * n),
        out_shape=jax.ShapeDtypeStruct((rows, cols), BF16),
        in_specs=[vmem, vmem, hbm, hbm, hbm, vmem, hbm, hbm, hbm],
        out_specs=vmem,
        scratch_shapes=[
            pltpu.VMEM((3, 2, 2, quarter, cols), BF16),
            pltpu.VMEM((2, 2, half, cols), BF16),
            pltpu.VMEM((2, chunks, cols, 2 * w), BF16),
            pltpu.VMEM((2, chunks, w, cols), BF16),
            pltpu.VMEM((2, 2, chunks, half, 2 * w), BF16),
            pltpu.VMEM((2, 2, chunks, half, 2 * w), BF16),
            pltpu.VMEM((2, 2, chunks, half, w), BF16),
            pltpu.VMEM((2, 2, 8, 128), F32),
            pltpu.VMEM((2, 2, n, 8, 128), F32),
            pltpu.VMEM((2, 2, half, 128), F32),
            pltpu.VMEM((2, 2, 2, quarter, cols), F32),
            pltpu.VMEM((2, 2, quarter, cols), F32),
            pltpu.VMEM((2, nx, 2, quarter, cols), BF16),
            dma((2, chunks)), dma((2,)),
            dma((2, 2)), dma((2, 2, chunks)),
            dma((2, 2)), dma((2, 2, n)),
            dma((2, 2, odd)), dma((2, 2)), dma((2, 2, chunks)),
            dma((2, 2)), dma((2, 2)),
            dma((2, max(nx - 1, 1), 2)), dma((2, max(nx - 1, 1), 2)),
            dma((2, 2)), dma((2, 2)),
        ],
        compiler_params=pltpu.CompilerParams(collective_id=0, has_side_effects=True),
    )(
        x, gain1, gate1, up1, down1.reshape(chunks, w, cols),
        gain2, gate2, up2, down2.reshape(chunks, w, cols),
    )


def solution(mesh):
    placed = (
        P("grp", "ra"),
        P("ra"),
        P("ra", "cb"),
        P("ra", "cb"),
        P("cb", "ra"),
        P("ra"),
        P("ra", "cb"),
        P("ra", "cb"),
        P("cb", "ra"),
    )
    body = functools.partial(per_device, mesh.shape["ra"], mesh.shape["cb"])
    return jax.shard_map(
        body, mesh=mesh, in_specs=placed, out_specs=P("grp", "ra"), check_vma=False
    )
```

time: 66.9 us -> 63 us (0.942); the launches traced: 65.8 us -> 62.8 us
  local copies, waits for them, and re-layouts: 4.09 us -> 1.57 us
    reshape x2 -> x0, local copies, waits for them, and re-layouts: 2.53 us -> none  [the longest x1 1.27 us: per_device(): gain2.reshape(1, cols)]
where the time goes in v2:
time: 63 us; the launch traced here: 62.8 us
  Pallas kernels  61.3 us (97%)
  local copies, waits for them, and re-layouts  1.57 us (2%)
    pallas_call x1, Pallas kernels, per_device(): pl.pallas_call(functools.partial(kernel, n, m, chunks, w, half, cols * n)...  61.3 us
    unnamed x1, local copies, waits for them, and re-layouts  1.57 us

profile of v2, /device:TPU:0, one launch (start us, length us, event | category | flops | bytes accessed | tf_op | source)
XLA Modules:
  0.0 62.8 jit_solution(922880220901604240)
XLA Ops:
  0.0 61.3 %shard_map.91 = bf16[128,512]{1,0:T(8,128)(2,1)} custom-call(bf16[128,512]{1,0:T(8,128)(2,1)} %x_ref.1, bf16[512]{0:T(512)(128)(2,1)} %gain1.1, bf16[512,1408]{1,0:T(8,128)(2,1)} %gate1.1, bf16[512,1408]{1,0:T(8,128)(2,1)} %up1.1, bf16[11,128,512]{2,1,0:T(8,128)(2,1)} %bitcast.2, bf16[512]{0:T(512)(128)(2,1)} %gain2.1, bf16[512,1408]{1,0:T(8,128)(2,1)} %gate2.1, ...), custom_call_target="tpu_custom_call" | custom-call | tf_op jit(solution)/shard_map/pallas_call | solution.py:319
  61.3 1.6 %copy.11 = bf16[128,512]{1,0:T(8,128)(2,1)} copy(bf16[128,512]{1,0:T(8,128)(2,1)} %shard_map.91) | data formatting | bytes 262144
